TPU v7x, 32 devices: a whole 2x2x4 slice. The times are simulated.
32 devices in a mesh: fs: 8 (over z, y), tp: 4 (over x, core).
Axes of the slice: x: 2, y: 2, z: 4, core: 2. Of those that a mesh axis runs over, the one named last changes fastest.
Arguments:
- tokens: bfloat16 [3072, 2048], P('fs'), may hold values from -6 to 6
- norm_gain: float32 [2048], replicated, may hold values from 0.1 to 1.9
- w_gate: bfloat16 [2048, 4096], P('fs', 'tp'), may hold values from -0.125 to 0.125
- w_up: bfloat16 [2048, 4096], P('fs', 'tp'), may hold values from -0.125 to 0.125
- w_down: bfloat16 [4096, 2048], P('tp', 'fs'), may hold values from -0.09375 to 0.09375
- cotangent: bfloat16 [3072, 2048], P('fs'), may hold values from -6 to 6
Outputs:
- grad_tokens: bfloat16 [3072, 2048], P('fs')
- grad_down: float32 [4096, 2048], P('tp', 'fs')
- down_norms: float32 [4096], P('tp')
All inputs are finite; a program needn't handle non-finite values.
Results may differ from a plain program's by a relative error of at most 0.018.
Values may be sent and summed in bfloat16 or wider, within the bound.
A program may use at most 64 MiB of HBM per device.

v0:
```python
import jax
import jax.numpy as jnp
from jax import lax
from jax.sharding import PartitionSpec as P

EPS = 1e-06


def shards(tokens, norm_gain, w_gate, w_up, w_down, cotangent):
    xf = tokens.astype(jnp.float32)
    inv = lax.rsqrt(jnp.mean(xf * xf, axis=-1, keepdims=True) + EPS)
    scaled = xf * inv
    normed = (scaled * norm_gain).astype(jnp.bfloat16)
    full_gate, full_up = (
        lax.all_gather(w_gate, "fs", axis=0, tiled=True),
        lax.all_gather(w_up, "fs", axis=0, tiled=True),
    )
    gate = jnp.dot(normed, full_gate, preferred_element_type=jnp.float32)
    up = jnp.dot(normed, full_up, preferred_element_type=jnp.float32)
    full_down = lax.all_gather(w_down, "fs", axis=1, tiled=True)
    d_hidden = 0.5 * lax.dot_general(
        cotangent, full_down, (((1,), (1,)), ((), ())), preferred_element_type=jnp.float32
    )
    sig = jax.nn.sigmoid(gate)
    act = gate * sig
    hidden = (act * up).astype(jnp.bfloat16)
    share = lax.psum_scatter(
        0.5
        * lax.dot_general(
            cotangent, hidden, (((0,), (0,)), ((), ())), preferred_element_type=jnp.float32
        ),
        "fs",
        scatter_dimension=0,
        tiled=True,
    )
    grad_down = share.T
    down_norms = lax.psum(jnp.sum(share * share, axis=0), "fs")
    d_gate = (d_hidden * up * sig * (1.0 + gate * (1.0 - sig))).astype(jnp.bfloat16)
    d_up = (d_hidden * act).astype(jnp.bfloat16)
    part = lax.dot_general(
        d_gate, full_gate, (((1,), (1,)), ((), ())), preferred_element_type=jnp.float32
    )
    part = part + lax.dot_general(
        d_up, full_up, (((1,), (1,)), ((), ())), preferred_element_type=jnp.float32
    )
    d_normed = lax.psum(part.astype(jnp.bfloat16), "tp").astype(jnp.float32)
    d_scaled = d_normed * norm_gain
    inner = jnp.mean(d_scaled * scaled, axis=-1, keepdims=True)
    grad_tokens = (inv * (d_scaled - scaled * inner)).astype(jnp.bfloat16)
    return (grad_tokens, grad_down, down_norms)


def solution(mesh):
    in_specs = (P("fs", None), P(), P("fs", "tp"), P("fs", "tp"), P("tp", "fs"), P("fs", None))
    out_specs = (P("fs", None), P("tp", "fs"), P("tp"))
    return jax.shard_map(shards, mesh=mesh, in_specs=in_specs, out_specs=out_specs, check_vma=False)
```

profile of v0, /device:TPU:0, one launch (start us, length us, event | category | flops | bytes accessed | tf_op | source)
XLA Modules:
  0.0 465.4 jit_solution(9571083893437479474)
XLA Ops:
  7.2 0.0 copy-start
  7.2 0.0 copy-start.1
  7.2 0.0 copy-start.3
  7.2 0.0 all-gather.8.cloned.1.call-start
  7.2 0.7 all-gather.8.cloned.1.call-update
  7.9 0.0 all-gather.6.cloned.1.call-start
  8.0 0.7 all-gather.6.cloned.1.call-update
  8.7 0.0 all-gather.4.cloned.1.call-start
  8.7 0.7 all-gather.4.cloned.1.call-update
  9.4 0.0 all-reduce.2.cloned.1.call-start
  9.5 1.8 fusion.8
  11.3 74.4 %all-gather.8.cloned.1.call-done = bf16[2048,1024]{1,0:T(8,128)(2,1)} async-done(((bf16[256,1024]{1,0:T(8,128)(2,1)}), bf16[2048,1024]{1,0:T(8,128)(2,1)}) %all-gather.8.cloned.1.call-update) | async-done | bytes 4194320 | tf_op jit(solution)/shard_map/all_gather | solution.py:15
  85.7 0.0 copy-done.1
  85.7 0.0 copy-done.3
  85.7 5.2 %fusion.12 = f32[384,1024]{1,0:T(8,128)} fusion(bf16[2048,1024]{1,0:T(8,128)(2,1)} %all-gather.8.cloned.1.call-done, bf16[384,2048]{1,0:T(8,128)(2,1)S(1)} %copy-done.1, f32[2048]{0:T(1024)S(1)} %copy-done.3, f32[384]{0:T(512)S(1)} %add_rsqrt_fusion), kind=kOutput, calls=%fused_computation.23 | convolution fusion | flops 1613758464 | bytes 7349760 | tf_op jit(solution)/shard_map/dot_general | solution.py:18
  90.9 68.3 %all-gather.6.cloned.1.call-done = bf16[2048,1024]{1,0:T(8,128)(2,1)} async-done(((bf16[256,1024]{1,0:T(8,128)(2,1)}), bf16[2048,1024]{1,0:T(8,128)(2,1)}) %all-gather.6.cloned.1.call-update) | async-done | bytes 4194320 | tf_op jit(solution)/shard_map/all_gather | solution.py:16
  159.2 5.2 %fusion.14 = f32[384,1024]{1,0:T(8,128)} fusion(bf16[2048,1024]{1,0:T(8,128)(2,1)} %all-gather.6.cloned.1.call-done, bf16[384,2048]{1,0:T(8,128)(2,1)S(1)} %copy-done.1, f32[2048]{0:T(1024)S(1)} %copy-done.3, f32[384]{0:T(512)S(1)} %add_rsqrt_fusion), kind=kOutput, calls=%fused_computation.24 | convolution fusion | flops 1613758464 | bytes 7349760 | tf_op jit(solution)/shard_map/dot_general | solution.py:19
  164.4 70.0 %all-gather.4.cloned.1.call-done = bf16[1024,2048]{1,0:T(8,128)(2,1)} async-done(((bf16[1024,256]{1,0:T(8,128)(2,1)}), bf16[1024,2048]{1,0:T(8,128)(2,1)}) %all-gather.4.cloned.1.call-update) | async-done | bytes 4194320 | tf_op jit(solution)/shard_map/all_gather | solution.py:20
  234.4 0.0 copy-done
  234.4 0.0 copy-start.4
  234.4 0.0 copy-start.6
  234.4 0.0 copy-start.7
  234.4 4.2 convolution_multiply_fusion
  238.6 0.0 copy-done.4
  238.6 0.0 copy-done.6
  238.6 0.2 copy-done.7
  238.8 0.0 copy-start.5
  238.8 2.3 fusion.10
  241.1 0.0 copy-done.5
  241.1 3.0 add_convert_fusion
  244.1 0.0 all-reduce.2.cloned.1.call-update
  244.1 0.2 reduce-scatter.2.cloned.1.call-start
  244.4 7.5 %multiply_bitcast_fusion = f32[2048,1024]{0,1:T(8,128)} fusion(bf16[384,2048]{1,0:T(8,128)(2,1)S(1)} %copy-done, f32[384,1024]{1,0:T(8,128)} %fusion.14, f32[384,1024]{1,0:T(8,128)} %fusion.12), kind=kOutput, calls=%fused_computation | convolution fusion | flops 1615069184 | bytes 13107200 | tf_op jit(solution)/shard_map/dot_general | solution.py:29
  251.9 0.0 reduce-scatter.2.cloned.1.call-update
  251.9 33.4 %all-reduce.2.cloned.1.call-done = bf16[384,2048]{1,0:T(8,128)(2,1)} async-done(((bf16[384,2048]{1,0:T(8,128)(2,1)}), bf16[384,2048]{1,0:T(8,128)(2,1)}) %all-reduce.2.cloned.1.call-update) | async-done | bytes 1572880 | tf_op jit(solution)/shard_map/psum | solution.py:46
  285.3 0.0 copy-start.2
  285.3 2.3 fusion.4
  287.6 0.0 copy-done.2
  287.6 2.0 fusion.7
  289.6 147.7 %reduce-scatter.2.cloned.1.call-done = f32[256,1024]{0,1:T(8,128)} async-done(((f32[2048,1024]{0,1:T(8,128)}), f32[256,1024]{0,1:T(8,128)}) %reduce-scatter.2.cloned.1.call-update) | async-done | bytes 1048592 | tf_op jit(solution)/shard_map/reduce_scatter | solution.py:27
  437.3 1.4 multiply_reduce_fusion
  438.8 20.1 %psum.15 = f32[1024]{0:T(1024)} all-reduce(f32[1024]{0:T(1024)S(1)} %multiply_reduce_fusion), channel_id=1, replica_groups=mesh['fs'=8,'tp'=4] {'fs'}, use_global_device_ids=true, to_apply=%region_5.0 | all-reduce | flops 1024 | bytes 8192 | tf_op jit(solution)/shard_map/psum | solution.py:37
  (2 shorter events, 0.0 us)
Async XLA Ops:
  7.2 227.3 %copy-start = (bf16[384,2048]{1,0:T(8,128)(2,1)S(1)}, bf16[384,2048]{1,0:T(8,128)(2,1)}, u32[]{:S(2)}) copy-start(bf16[384,2048]{1,0:T(8,128)(2,1)} %param.11) | copy-start | bytes 4718596
  7.2 78.5 %copy-start.1 = (bf16[384,2048]{1,0:T(8,128)(2,1)S(1)}, bf16[384,2048]{1,0:T(8,128)(2,1)}, u32[]{:S(2)}) copy-start(bf16[384,2048]{1,0:T(8,128)(2,1)} %param.6) | copy-start | bytes 4718596
  7.2 78.5 %copy-start.3 = (f32[2048]{0:T(1024)S(1)}, f32[2048]{0:T(1024)}, u32[]{:S(2)}) copy-start(f32[2048]{0:T(1024)} %param.7) | copy-start | bytes 24580
  7.2 78.5 %all-gather.8.cloned.1.call-start = ((), (), s32[]{:S(2)}) async-start(), calls=%async_computation.3 | async-start | bytes 4718592 | tf_op jit(solution)/shard_map/all_gather | solution.py:15
  7.9 151.2 %all-gather.6.cloned.1.call-start = ((), (), s32[]{:S(2)}) async-start(), calls=%async_computation.2 | async-start | bytes 4718592 | tf_op jit(solution)/shard_map/all_gather | solution.py:16
  8.7 225.7 %all-gather.4.cloned.1.call-start = ((), (), s32[]{:S(2)}) async-start(), calls=%async_computation.1 | async-start | bytes 4718592 | tf_op jit(solution)/shard_map/all_gather | solution.py:20
  9.4 275.9 %all-reduce.2.cloned.1.call-start = ((), (), s32[]{:S(2)}) async-start(), calls=%async_computation.4 | async-start | bytes 3145728 | tf_op jit(solution)/shard_map/psum | solution.py:46
  234.4 4.2 copy-start.4
  234.4 4.2 copy-start.6
  234.4 4.4 copy-start.7
  238.8 2.3 copy-start.5
  244.1 193.2 %reduce-scatter.2.cloned.1.call-start = ((), (), s32[]{:S(2)}) async-start(), calls=%async_computation.5 | async-start | bytes 9437184 | tf_op jit(solution)/shard_map/reduce_scatter | solution.py:27
  285.3 2.3 copy-start.2
Sparse Core Ops, SparseCore 0:
  10.1 75.5 all-gather.7
  87.8 71.3 all-gather.5
  161.2 73.1 all-gather.3
  244.2 41.0 all-reduce.1
  289.4 147.9 reduce-scatter.1
where the time goes:
time: 466 us; the launch traced here: 465 us
  waiting for transfers between devices  396 us (85%)
  matrix products  27.3 us (6%)
  blocking collectives  20.1 us (4%)
  between operations  13.9 us (3%)
  other arithmetic  7.55 us (2%)
    reduce_scatter x1, waiting for transfers between devices, shards(): lax.psum_scatter(0.5 * lax.dot_general(cotangent, hidden, (((0,), (0,)),...  148 us
    all_gather x1, waiting for transfers between devices, shards(): lax.all_gather(w_gate, 'fs', axis=0, tiled=True)  74.4 us
    all_gather x1, waiting for transfers between devices, shards(): full_down = lax.all_gather(w_down, 'fs', axis=1, tiled=True)  70 us
    all_gather x1, waiting for transfers between devices, shards(): lax.all_gather(w_up, 'fs', axis=0, tiled=True)  68.3 us
    psum x1, waiting for transfers between devices, shards(): d_normed = lax.psum(part.astype(jnp.bfloat16), 'tp').astype(jnp.float32)  33.4 us
    psum x1, blocking collectives, shards(): down_norms = lax.psum(jnp.sum(share * share, axis=0), 'fs')  20.1 us
  transfers between devices with their start and end apart: 5, of which 5 were waited for; matrix products, arithmetic and copies ran while one was open for 5% of the time, Pallas kernels for 0%

commit v1 on v0

--- a/solution.py
+++ b/solution.py
@@ -7,6 +7,20 @@
 
 
 def shards(tokens, norm_gain, w_gate, w_up, w_down, cotangent):
+
+    def view_links(mesh_name, obj):
+        n_parts = lax.axis_size(mesh_name)
+        big = sorted(((i0, (i0 + 1) % n_parts) for i0 in range(n_parts)))
+        mixed_arr = obj
+        stack_in = [mixed_arr]
+        for at in range(1, n_parts):
+            mixed_arr = lax.ppermute(mixed_arr, mesh_name, big)
+            stack_in.insert(0, mixed_arr)
+        tall = jnp.concatenate(stack_in, axis=1)
+        t_next = lax.axis_index(mesh_name) + 1
+        local_out = jnp.roll(tall, t_next * obj.shape[1], axis=1)
+        return local_out
+
     xf = tokens.astype(jnp.float32)
     inv = lax.rsqrt(jnp.mean(xf * xf, axis=-1, keepdims=True) + EPS)
     scaled = xf * inv
@@ -17,7 +31,7 @@
     )
     gate = jnp.dot(normed, full_gate, preferred_element_type=jnp.float32)
     up = jnp.dot(normed, full_up, preferred_element_type=jnp.float32)
-    full_down = lax.all_gather(w_down, "fs", axis=1, tiled=True)
+    full_down = view_links("fs", w_down)
     d_hidden = 0.5 * lax.dot_general(
         cotangent, full_down, (((1,), (1,)), ((), ())), preferred_element_type=jnp.float32
     )

time: 466 us -> 440 us (0.944)
  waiting for transfers between devices: 396 us -> 359 us
  local copies, waits for them, and re-layouts: 0.24 us -> 7.33 us
    ppermute x0 -> x7, waiting for transfers between devices: none -> 153 us  [view_links(): mixed_arr = lax.ppermute(mixed_arr, mesh_name, big)]
    all_gather x1, waiting for transfers between devices: 74.4 us -> 0.01 us  [shards(): lax.all_gather(w_gate, 'fs', axis=0, tiled=True)]
    all_gather x1 -> x0, waiting for transfers between devices: 70 us -> none  [shards(): full_down = lax.all_gather(w_down, 'fs', axis=1, tiled=True)]
    all_gather x1, waiting for transfers between devices: 68.3 us -> 23.3 us  [shards(): lax.all_gather(w_up, 'fs', axis=0, tiled=True)]
    unnamed x16 -> x43, local copies, waits for them, and re-layouts: 0.24 us -> 7.27 us
  transfers between devices with their start and end apart: 5 -> 11, of which waited for: 5 -> 10; matrix products, arithmetic and copies ran while one was open for 5% -> 6% of each run, Pallas kernels for 0% -> 0%
where the time goes in v1:
time: 440 us; the launch traced here: 439 us
  waiting for transfers between devices  359 us (82%)
  matrix products  26.9 us (6%)
  blocking collectives  20.1 us (5%)
  between operations  14 us (3%)
  other arithmetic  7.61 us (2%)
  local copies, waits for them, and re-layouts  7.33 us (2%)
    ppermute x7, waiting for transfers between devices, view_links(): mixed_arr = lax.ppermute(mixed_arr, mesh_name, big)  153 us
    reduce_scatter x1, waiting for transfers between devices, shards(): lax.psum_scatter(0.5 * lax.dot_general(cotangent, hidden, (((0,), (0,)),...  148 us
    psum x1, waiting for transfers between devices, shards(): d_normed = lax.psum(part.astype(jnp.bfloat16), 'tp').astype(jnp.float32)  33.8 us
    all_gather x1, waiting for transfers between devices, shards(): lax.all_gather(w_up, 'fs', axis=0, tiled=True)  23.3 us
    psum x1, blocking collectives, shards(): down_norms = lax.psum(jnp.sum(share * share, axis=0), 'fs')  20.1 us
  transfers between devices with their start and end apart: 11, of which 10 were waited for; matrix products, arithmetic and copies ran while one was open for 6% of the time, Pallas kernels for 0%

profile of v1, /device:TPU:0, one launch (start us, length us, event | category | flops | bytes accessed | tf_op | source)
XLA Modules:
  0.0 439.3 jit_solution(16170239079108986037)
XLA Ops:
  7.2 0.0 copy-start
  7.2 0.0 all-gather.5.cloned.1.call-start
  7.2 0.7 all-gather.5.cloned.1.call-update
  7.9 0.0 all-gather.3.cloned.1.call-start
  8.0 0.7 all-gather.3.cloned.1.call-update
  8.7 0.0 all-reduce.2.cloned.1.call-start
  8.7 3.0 collective-permute-start
  11.8 15.7 %collective-permute-done = bf16[1024,256]{1,0:T(8,128)(2,1)S(1)} collective-permute-done((bf16[1024,256]{1,0:T(8,128)(2,1)}, bf16[1024,256]{1,0:T(8,128)(2,1)S(1)}, u32[]{:S(2)}, u32[]{:S(2)}) %collective-permute-start) | collective-permute-done | bytes 524320 | tf_op jit(solution)/shard_map/ppermute | solution.py:17
  27.5 1.0 collective-permute-start.1
  28.4 26.6 %collective-permute-done.1 = bf16[1024,256]{1,0:T(8,128)(2,1)S(1)} collective-permute-done((bf16[1024,256]{1,0:T(8,128)(2,1)S(1)}, bf16[1024,256]{1,0:T(8,128)(2,1)S(1)}, u32[]{:S(2)}, u32[]{:S(2)}) %collective-permute-start.1) | collective-permute-done | bytes 524320 | tf_op jit(solution)/shard_map/ppermute | solution.py:17
  55.1 0.0 collective-permute-start.2
  55.1 25.6 %collective-permute-done.2 = bf16[1024,256]{1,0:T(8,128)(2,1)S(1)} collective-permute-done((bf16[1024,256]{1,0:T(8,128)(2,1)S(1)}, bf16[1024,256]{1,0:T(8,128)(2,1)S(1)}, u32[]{:S(2)}, u32[]{:S(2)}) %collective-permute-start.2) | collective-permute-done | bytes 524320 | tf_op jit(solution)/shard_map/ppermute | solution.py:17
  80.7 0.0 collective-permute-start.3
  80.7 26.7 %collective-permute-done.3 = bf16[1024,256]{1,0:T(8,128)(2,1)S(1)} collective-permute-done((bf16[1024,256]{1,0:T(8,128)(2,1)S(1)}, bf16[1024,256]{1,0:T(8,128)(2,1)S(1)}, u32[]{:S(2)}, u32[]{:S(2)}) %collective-permute-start.3) | collective-permute-done | bytes 524320 | tf_op jit(solution)/shard_map/ppermute | solution.py:17
  107.3 0.8 copy-done.4
  108.1 0.0 collective-permute-start.4
  108.1 18.2 %collective-permute-done.4 = bf16[1024,256]{1,0:T(8,128)(2,1)S(1)} collective-permute-done((bf16[1024,256]{1,0:T(8,128)(2,1)S(1)}, bf16[1024,256]{1,0:T(8,128)(2,1)S(1)}, u32[]{:S(2)}, u32[]{:S(2)}) %collective-permute-start.4) | collective-permute-done | bytes 524320 | tf_op jit(solution)/shard_map/ppermute | solution.py:17
  126.3 0.8 copy-done.6
  127.1 0.0 collective-permute-start.5
  127.1 24.4 %collective-permute-done.5 = bf16[1024,256]{1,0:T(8,128)(2,1)} collective-permute-done((bf16[1024,256]{1,0:T(8,128)(2,1)S(1)}, bf16[1024,256]{1,0:T(8,128)(2,1)}, u32[]{:S(2)}, u32[]{:S(2)}) %collective-permute-start.5) | collective-permute-done | bytes 524320 | tf_op jit(solution)/shard_map/ppermute | solution.py:17
  151.4 0.0 collective-permute-start.6
  151.4 1.9 fusion.10
  153.3 15.5 %collective-permute-done.6 = bf16[1024,256]{1,0:T(8,128)(2,1)} collective-permute-done((bf16[1024,256]{1,0:T(8,128)(2,1)}, bf16[1024,256]{1,0:T(8,128)(2,1)}, u32[]{:S(2)}, u32[]{:S(2)}) %collective-permute-start.6) | collective-permute-done | bytes 524320 | tf_op jit(solution)/shard_map/ppermute | solution.py:17
  168.9 1.1 constant_dynamic-update-slice_fusion.15
  170.0 0.0 copy-start.3
  170.0 1.2 constant_dynamic-update-slice_fusion.14
  171.2 0.1 constant_dynamic-update-slice_fusion.13
  171.2 0.0 copy-done.5
  171.2 0.1 constant_dynamic-update-slice_fusion.12
  171.3 0.1 constant_dynamic-update-slice_fusion.11
  171.4 0.1 constant_dynamic-update-slice_fusion.10
  171.5 0.1 constant_dynamic-update-slice_fusion.9
  171.5 0.1 constant_dynamic-update-slice_fusion.8
  171.6 1.1 constant_dynamic-update-slice_fusion.7
  172.7 1.1 constant_dynamic-update-slice_fusion.6
  173.8 0.1 constant_dynamic-update-slice_fusion.5
  173.9 0.1 constant_dynamic-update-slice_fusion.4
  174.0 0.1 constant_dynamic-update-slice_fusion.3
  174.1 0.1 constant_dynamic-update-slice_fusion.2
  174.1 0.1 constant_dynamic-update-slice_fusion.1
  174.2 0.1 constant_dynamic-update-slice_fusion
  174.3 0.0 copy-start.1
  174.3 0.0 copy-start.8
  174.3 3.5 fusion.16
  177.8 0.0 copy-done.8
  177.8 5.8 %fusion.23 = f32[384,1024]{0,1:T(8,128)} fusion(bf16[2048,1024]{1,0:T(8,128)(2,1)} %all-gather.5.cloned.1.call-done, bf16[384,2048]{1,0:T(8,128)(2,1)S(1)} %copy-done.1, f32[2048]{0:T(1024)S(1)} %copy-done.8, f32[384]{0:T(512)S(1)} %add_rsqrt_fusion), kind=kOutput, calls=%fused_computation.29 | convolution fusion | flops 1613758464 | bytes 7349760 | tf_op jit(solution)/shard_map/dot_general | solution.py:32
  183.7 23.3 %all-gather.3.cloned.1.call-done = bf16[2048,1024]{1,0:T(8,128)(2,1)} async-done(((bf16[256,1024]{1,0:T(8,128)(2,1)}), bf16[2048,1024]{1,0:T(8,128)(2,1)}) %all-gather.3.cloned.1.call-update) | async-done | bytes 4194320 | tf_op jit(solution)/shard_map/all_gather | solution.py:30
  207.0 4.8 %fusion.25 = f32[384,1024]{0,1:T(8,128)S(1)} fusion(bf16[2048,1024]{1,0:T(8,128)(2,1)} %all-gather.3.cloned.1.call-done, bf16[384,2048]{1,0:T(8,128)(2,1)S(1)} %copy-done.1, f32[2048]{0:T(1024)S(1)} %copy-done.8, f32[384]{0:T(512)S(1)} %add_rsqrt_fusion), kind=kOutput, calls=%fused_computation.30 | convolution fusion | flops 1613758464 | bytes 7349760 | tf_op jit(solution)/shard_map/dot_general | solution.py:33
  211.8 0.0 copy-done.9
  211.8 0.0 copy-done.11
  211.8 0.0 copy-done.13
  211.8 2.3 fusion.20
  214.1 0.4 copy-done.10
  214.6 3.1 add_convert_fusion
  217.6 0.0 all-reduce.2.cloned.1.call-update
  217.6 0.2 reduce-scatter.2.cloned.1.call-start
  217.9 7.5 %multiply_bitcast_fusion = f32[2048,1024]{0,1:T(8,128)} fusion(bf16[384,2048]{1,0:T(8,128)(2,1)S(1)} %copy-done, f32[384,1024]{0,1:T(8,128)} %copy-done.12, f32[384,1024]{0,1:T(8,128)} %fusion.23), kind=kOutput, calls=%fused_computation | convolution fusion | flops 1615069184 | bytes 13107200 | tf_op jit(solution)/shard_map/dot_general | solution.py:43
  225.3 0.0 reduce-scatter.2.cloned.1.call-update
  225.4 33.8 %all-reduce.2.cloned.1.call-done = bf16[384,2048]{1,0:T(8,128)(2,1)} async-done(((bf16[384,2048]{1,0:T(8,128)(2,1)}), bf16[384,2048]{1,0:T(8,128)(2,1)}) %all-reduce.2.cloned.1.call-update) | async-done | bytes 1572880 | tf_op jit(solution)/shard_map/psum | solution.py:60
  259.2 2.3 fusion.6
  261.5 2.0 fusion.9
  263.5 147.7 %reduce-scatter.2.cloned.1.call-done = f32[256,1024]{0,1:T(8,128)} async-done(((f32[2048,1024]{0,1:T(8,128)}), f32[256,1024]{0,1:T(8,128)}) %reduce-scatter.2.cloned.1.call-update) | async-done | bytes 1048592 | tf_op jit(solution)/shard_map/reduce_scatter | solution.py:41
  411.2 1.4 multiply_reduce_fusion
  412.7 20.1 %psum.15 = f32[1024]{0:T(1024)} all-reduce(f32[1024]{0:T(1024)S(1)} %multiply_reduce_fusion), channel_id=1, replica_groups=mesh['fs'=8,'tp'=4] {'fs'}, use_global_device_ids=true, to_apply=%region_5.6 | all-reduce | flops 1024 | bytes 8192 | tf_op jit(solution)/shard_map/psum | solution.py:51
  (19 shorter events, 0.0 us)
Async XLA Ops:
  7.2 167.1 %copy-start = (bf16[384,2048]{1,0:T(8,128)(2,1)S(1)}, bf16[384,2048]{1,0:T(8,128)(2,1)}, u32[]{:S(2)}) copy-start(bf16[384,2048]{1,0:T(8,128)(2,1)} %param.11) | copy-start | bytes 4718596
  7.2 170.6 %all-gather.5.cloned.1.call-start = ((), (), s32[]{:S(2)}) async-start(), calls=%async_computation.2 | async-start | bytes 4718592 | tf_op jit(solution)/shard_map/all_gather | solution.py:29
  7.9 199.1 %all-gather.3.cloned.1.call-start = ((), (), s32[]{:S(2)}) async-start(), calls=%async_computation.1 | async-start | bytes 4718592 | tf_op jit(solution)/shard_map/all_gather | solution.py:30
  8.7 250.5 %all-reduce.2.cloned.1.call-start = ((), (), s32[]{:S(2)}) async-start(), calls=%async_computation.3 | async-start | bytes 3145728 | tf_op jit(solution)/shard_map/psum | solution.py:60
  8.7 18.8 %collective-permute-start = (bf16[1024,256]{1,0:T(8,128)(2,1)}, bf16[1024,256]{1,0:T(8,128)(2,1)S(1)}, u32[]{:S(2)}, u32[]{:S(2)}) collective-permute-start(bf16[1024,256]{1,0:T(8,128)(2,1)} %param.10), channel_id=1, source_target_pairs={{0,4},{4,8},{8,12},{12,16},{16,20},{20,24},{24,28},{28,0},{1,5},{5... | collective-permute-start | bytes 1572872 | tf_op jit(solution)/shard_map/ppermute | solution.py:17
  27.5 27.6 %collective-permute-start.1 = (bf16[1024,256]{1,0:T(8,128)(2,1)S(1)}, bf16[1024,256]{1,0:T(8,128)(2,1)S(1)}, u32[]{:S(2)}, u32[]{:S(2)}) collective-permute-start(bf16[1024,256]{1,0:T(8,128)(2,1)S(1)} %collective-permute-done), channel_id=1, source_target_pairs={{0,4},{4,8},{8,12},{12,16},{16,20},{20,24},{24,28},{28,0},{1,5},{5... | collective-permute-start | bytes 1572872 | tf_op jit(solution)/shard_map/ppermute | solution.py:17
  55.1 25.6 %collective-permute-start.2 = (bf16[1024,256]{1,0:T(8,128)(2,1)S(1)}, bf16[1024,256]{1,0:T(8,128)(2,1)S(1)}, u32[]{:S(2)}, u32[]{:S(2)}) collective-permute-start(bf16[1024,256]{1,0:T(8,128)(2,1)S(1)} %collective-permute-done.1), channel_id=1, source_target_pairs={{0,4},{4,8},{8,12},{12,16},{16,20},{20,24},{24,28},{28,0},{1,5},{5... | collective-permute-start | bytes 1572872 | tf_op jit(solution)/shard_map/ppermute | solution.py:17
  80.7 26.7 %collective-permute-start.3 = (bf16[1024,256]{1,0:T(8,128)(2,1)S(1)}, bf16[1024,256]{1,0:T(8,128)(2,1)S(1)}, u32[]{:S(2)}, u32[]{:S(2)}) collective-permute-start(bf16[1024,256]{1,0:T(8,128)(2,1)S(1)} %collective-permute-done.2), channel_id=1, source_target_pairs={{0,4},{4,8},{8,12},{12,16},{16,20},{20,24},{24,28},{28,0},{1,5},{5... | collective-permute-start | bytes 1572872 | tf_op jit(solution)/shard_map/ppermute | solution.py:17
  107.3 0.8 copy-start.4
  108.1 18.2 %collective-permute-start.4 = (bf16[1024,256]{1,0:T(8,128)(2,1)S(1)}, bf16[1024,256]{1,0:T(8,128)(2,1)S(1)}, u32[]{:S(2)}, u32[]{:S(2)}) collective-permute-start(bf16[1024,256]{1,0:T(8,128)(2,1)S(1)} %collective-permute-done.3), channel_id=1, source_target_pairs={{0,4},{4,8},{8,12},{12,16},{16,20},{20,24},{24,28},{28,0},{1,5},{5... | collective-permute-start | bytes 1572872 | tf_op jit(solution)/shard_map/ppermute | solution.py:17
  126.3 0.8 copy-start.6
  127.1 24.4 %collective-permute-start.5 = (bf16[1024,256]{1,0:T(8,128)(2,1)S(1)}, bf16[1024,256]{1,0:T(8,128)(2,1)}, u32[]{:S(2)}, u32[]{:S(2)}) collective-permute-start(bf16[1024,256]{1,0:T(8,128)(2,1)S(1)} %collective-permute-done.4), channel_id=1, source_target_pairs={{0,4},{4,8},{8,12},{12,16},{16,20},{20,24},{24,28},{28,0},{1,5},{5... | collective-permute-start | bytes 1572872 | tf_op jit(solution)/shard_map/ppermute | solution.py:17
  151.4 17.4 %collective-permute-start.6 = (bf16[1024,256]{1,0:T(8,128)(2,1)}, bf16[1024,256]{1,0:T(8,128)(2,1)}, u32[]{:S(2)}, u32[]{:S(2)}) collective-permute-start(bf16[1024,256]{1,0:T(8,128)(2,1)} %collective-permute-done.5), channel_id=1, source_target_pairs={{0,4},{4,8},{8,12},{12,16},{16,20},{20,24},{24,28},{28,0},{1,5},{5... | collective-permute-start | bytes 1572872 | tf_op jit(solution)/shard_map/ppermute | solution.py:17
  151.4 19.7 %copy-start.7 = (bf16[1024,256]{1,0:T(8,128)(2,1)S(1)}, bf16[1024,256]{1,0:T(8,128)(2,1)}, u32[]{:S(2)}) copy-start(bf16[1024,256]{1,0:T(8,128)(2,1)} %copy-done.6) | copy-start | bytes 1572868
  151.4 19.8 %copy-start.5 = (bf16[1024,256]{1,0:T(8,128)(2,1)S(1)}, bf16[1024,256]{1,0:T(8,128)(2,1)}, u32[]{:S(2)}) copy-start(bf16[1024,256]{1,0:T(8,128)(2,1)} %copy-done.4) | copy-start | bytes 1572868
  170.0 1.6 copy-start.3
  174.3 3.5 copy-start.1
  174.3 3.5 copy-start.8
  207.0 4.8 %copy-start.9 = (bf16[2048,1024]{1,0:T(8,128)(2,1)S(1)}, bf16[2048,1024]{1,0:T(8,128)(2,1)}, u32[]{:S(2)}) copy-start(bf16[2048,1024]{1,0:T(8,128)(2,1)} %all-gather.5.cloned.1.call-done) | copy-start | bytes 12582916
  207.0 4.8 %copy-start.11 = (f32[384,1024]{0,1:T(8,128)S(1)}, f32[384,1024]{0,1:T(8,128)}, u32[]{:S(2)}) copy-start(f32[384,1024]{0,1:T(8,128)} %fusion.23) | copy-start | bytes 4718596
  207.0 4.8 %copy-start.13 = (f32[1024,384]{1,0:T(8,128)S(1)}, f32[1024,384]{1,0:T(8,128)}, u32[]{:S(2)}) copy-start(f32[1024,384]{1,0:T(8,128)} %fusion.16) | copy-start | bytes 4718596
  211.8 2.3 copy-start.12
  211.8 2.8 copy-start.10
  217.6 193.6 %reduce-scatter.2.cloned.1.call-start = ((), (), s32[]{:S(2)}) async-start(), calls=%async_computation.4 | async-start | bytes 9437184 | tf_op jit(solution)/shard_map/reduce_scatter | solution.py:41
  259.2 2.3 copy-start.2
Sparse Core Ops, SparseCore 0:
  10.1 104.3 all-gather.4
  116.6 90.3 all-gather.2
  217.8 41.3 all-reduce.1
  263.3 147.9 reduce-scatter.1
